TPU v7x, 32 devices: a whole 2x2x4 slice. The times are simulated.
32 devices in a mesh: grp: 2 (over y), fs: 4 (over z), tp: 4 (over x, core).
Axes of the slice: x: 2, y: 2, z: 4, core: 2. Of those that a mesh axis runs over, the one named last changes fastest.
Arguments:
- tokens: bfloat16 [1536, 2048], P(('grp', 'tp')), parts along dimension 0, may hold values from -6 to 6
- routes: int32 [1536, 2], P(('grp', 'tp')), parts along dimension 0, may hold values from 0 to 3, all different within a row; in each aligned block of 192 rows (0 to 191, 192 to 383, ...) at most 128 rows name the same one
- route_weight: float32 [1536, 2], P(('grp', 'tp')), parts along dimension 0, may hold values from 0.2 to 1
- norm_gain: float32 [2048], P('fs'), may hold values from 0.1 to 1.9
- gate_train: float32 [4, 2048, 5632], P('tp', 'fs'), may hold values from -0.125 to 0.125
- up_train: float32 [4, 2048, 5632], P('tp', 'fs'), may hold values from -0.125 to 0.125
- down_train: float32 [4, 5632, 2048], P('tp', None, 'fs'), may hold values from -0.109375 to 0.109375
Outputs:
- gate_serve: bfloat16 [8, 2048, 5632], P(('grp', 'tp'), None, 'fs'), parts along dimension 0
- up_serve: bfloat16 [8, 2048, 5632], P(('grp', 'tp'), None, 'fs'), parts along dimension 0
- down_serve: bfloat16 [8, 5632, 2048], P(('grp', 'tp'), 'fs'), parts along dimension 0
- mixed: bfloat16 [1536, 2048], P(('grp', 'tp'), 'fs'), parts along dimension 0
There are 2 independent parts, one for each index of `grp`. A program takes and returns all parts, laid end to end along the dimension named above; an argument that names none is the same for every part. Nothing has to cross between parts.
Inputs may be any that keep to these rules, and one draw needn't show every extreme that they name: `routes`: each row names 2 different experts. In each aligned block of 192 rows no expert is named by more than 128 rows, a bound that some block reaches.
All inputs are finite; a program needn't handle non-finite values.
Results may differ from a plain program's by a relative error of at most 0.0087.
Values may be sent and summed in bfloat16 or wider, within the bound.
A program may use at most 128 MiB of HBM per device.

v0:
```python
import functools
import jax
import jax.numpy as jnp
from jax import lax
from jax.experimental import pallas as pl
from jax.experimental.pallas import tpu as pltpu
from jax.sharding import PartitionSpec as P

EXPERTS = 4
CAP = 128
MESH = pl.DeviceIdType.MESH


def exchange_kernel(F, T, R, C, Q, gt, ut, dt, gain, tokens, routes_t, weight_t, gw, uw, dw, mo,
                    flat, turned, scale_at, wide, tall, sendw, sendt, normed, xs, bh, bl,
                    arr, gacc, uacc, hid, pbf, ret, msend, mown, mrecv,
                    zs, zr, ys, yr, ts, tr, ps, pr, ms, mr, loc):
    g, f, t = lax.axis_index("grp"), lax.axis_index("fs"), lax.axis_index("tp")
    H = R // 2
    wins = (gw, uw, dw)
    pieces_of = (1, 1, Q)
    half_f = F // 2
    lo = lax.div(f, half_f)
    peers = [lax.rem(t + d, T) for d in range(1, T)]
    others = [lo * k + (1 - lo) * (F - 1 - k) for k in range(half_f)]
    others += [lo * half_f + lax.rem(f - lo * half_f + 1 + j, half_f) for j in range(half_f - 1)]

    barrier = pltpu.get_barrier_semaphore()
    for p in peers:
        pl.semaphore_signal(barrier, inc=1, device_id={"tp": p}, device_id_type=MESH)
    for p in others:
        pl.semaphore_signal(barrier, inc=1, device_id={"fs": p}, device_id_type=MESH)
    pl.semaphore_signal(barrier, inc=1, device_id={"grp": 1 - g}, device_id_type=MESH)
    pl.semaphore_wait(barrier, len(peers) + len(others) + 1)

    def cols_of(src, half):
        return pl.ds(pl.multiple_of(src * R + half * H, H), H)

    def part(a, src, half, q):
        if a < 2:
            return wins[a].at[cols_of(src, half), :]
        return dw.at[pl.ds(q * (C // Q), C // Q), cols_of(src, half)]

    def z_copy(a, k, tgt, src, q):
        piece = sendw.at[a, k] if a < 2 else sendt.at[k, pl.ds(q * (C // Q), C // Q), :]
        return pltpu.make_async_remote_copy(
            src_ref=piece, dst_ref=part(a, src, g, q), send_sem=zs.at[a, k, q], recv_sem=zr.at[a, src, q],
            device_id={"fs": tgt}, device_id_type=MESH)

    def z_send(a, k):
        for q in range(pieces_of[a]):
            z_copy(a, k, others[k], f, q).start()

    def z_recv(a, src, q):
        return pltpu.make_async_remote_copy(
            src_ref=part(a, src, g, q), dst_ref=part(a, src, g, q), send_sem=zs.at[a, 0, q],
            recv_sem=zr.at[a, src, q], device_id={"fs": src}, device_id_type=MESH)

    def y_copy(a, src, half, q):
        return pltpu.make_async_remote_copy(
            src_ref=part(a, src, half, q), dst_ref=part(a, src, half, q), send_sem=ys.at[a, src, q],
            recv_sem=yr.at[a, src, q], device_id={"grp": 1 - g}, device_id_type=MESH)

    def slots(q):
        return pl.ds(pl.multiple_of(q * CAP, CAP), CAP)

    def t_copy(tgt, src):
        return pltpu.make_async_remote_copy(
            src_ref=xs.at[slots(tgt), :], dst_ref=arr.at[slots(src), :], send_sem=ts.at[tgt], recv_sem=tr.at[src],
            device_id={"tp": tgt}, device_id_type=MESH)

    def p_copy(c, half, tgt, src):
        cols = cols_of(c, half)
        return pltpu.make_async_remote_copy(
            src_ref=pbf.at[slots(tgt), cols], dst_ref=ret.at[slots(src), cols],
            send_sem=ps.at[c, half, tgt], recv_sem=pr.at[c, half, src],
            device_id={"tp": tgt}, device_id_type=MESH)

    def m_copy(tgt, half, src):
        return pltpu.make_async_remote_copy(
            src_ref=msend.at[:, cols_of(tgt, half)], dst_ref=mrecv.at[src, :, pl.ds(pl.multiple_of(half * H, H), H)],
            send_sem=ms.at[tgt, half], recv_sem=mr.at[src, half],
            device_id={"fs": tgt}, device_id_type=MESH)

    if len(others) == 3:
        order = [(0, 0), (0, 1), (0, 2), (1, 0), (1, 2), (2, 2), (1, 1), (2, 0), (2, 1)]
    else:
        order = [(a, k) for a in range(3) for k in range(len(others))]
    tasks = [(a, k, g) for a, k in order]
    tasks += [(a, None, half) for a in range(3) for half in range(2)]

    def stage_copy(n):
        a, k, half = tasks[n]
        tgt = f if k is None else others[k]
        near, far = pl.ds(pl.multiple_of(half * H, H), H), pl.ds(pl.multiple_of(tgt * C, C), C)
        if a < 2:
            return pltpu.make_async_copy((gt, ut)[a].at[near, far], wide.at[n % 3], loc.at[n % 3])
        return pltpu.make_async_copy(dt.at[far, near], tall.at[n % 3], loc.at[3 + n % 3])

    def cast(n):
        a, k, half = tasks[n]
        stage_copy(n).wait()
        if a < 2:
            @pl.loop(0, H // 32)
            def _(m):
                rows = pl.ds(pl.multiple_of(m * 32, 32), 32)
                scale = scale_at[pl.ds(pl.multiple_of(half * H + m * 32, 32), 32), 0:1]
                value = (wide[n % 3, rows, :] * scale).astype(jnp.bfloat16)
                if k is None:
                    wins[a][pl.ds(pl.multiple_of(f * R + half * H + m * 32, 32), 32), :] = value
                else:
                    sendw[a, k, rows, :] = value
        else:
            @pl.loop(0, C // 128)
            def _(m):
                rows = pl.ds(pl.multiple_of(m * 128, 128), 128)
                value = tall[n % 3, rows, :].astype(jnp.bfloat16)
                if k is None:
                    dw[rows, cols_of(f, half)] = value
                else:
                    sendt[k, rows, :] = value
        if n + 3 < len(tasks):
            stage_copy(n + 3).start()

    def route():
        tok, slot_all = tokens.shape[0], arr.shape[0]

        @pl.loop(0, tok // 32)
        def _(m):
            rows = pl.ds(pl.multiple_of(m * 32, 32), 32)
            value = tokens[rows, :].astype(jnp.float32)
            normed[rows, :] = (
                value * lax.rsqrt(jnp.mean(value * value, axis=-1, keepdims=True) + 1e-06)
            ).astype(jnp.bfloat16)

        one, two = routes_t[0:1, :], routes_t[1:2, :]
        row = lax.broadcasted_iota(jnp.int32, (tok, tok), 0)
        col = lax.broadcasted_iota(jnp.int32, (tok, tok), 1)
        expert = lax.broadcasted_iota(jnp.int32, (16, tok), 0)
        hot = jnp.where((expert == one) | (expert == two), 1.0, 0.0).astype(jnp.bfloat16)
        before = jnp.dot(hot, jnp.where(row < col, 1.0, 0.0).astype(jnp.bfloat16), preferred_element_type=jnp.float32)
        first, second = [
            name.astype(jnp.float32) * CAP
            + jnp.sum(jnp.where(expert == name, before, 0.0), axis=0, keepdims=True)
            for name in (one, two)
        ]
        slot = lax.broadcasted_iota(jnp.int32, (slot_all, tok), 0).astype(jnp.float32)
        select = jnp.where((slot == first) | (slot == second), 1.0, 0.0).astype(jnp.bfloat16)
        for n in range(4):
            cols = pl.ds(n * (F * R // 4), F * R // 4)
            xs[:, cols] = jnp.dot(select, normed[:, cols], preferred_element_type=jnp.float32).astype(jnp.bfloat16)
        flat[...] = jnp.zeros_like(flat)
        for n, line in enumerate((first, second, weight_t[0:1, :], weight_t[1:2, :])):
            flat[n:n + 1, 0:tok] = line
        turned[...] = flat[...].T
        slot = lax.broadcasted_iota(jnp.int32, (tok, slot_all), 1).astype(jnp.float32)
        blend = jnp.where(slot == turned[0:tok, 0:1], turned[0:tok, 2:3], 0.0) + jnp.where(
            slot == turned[0:tok, 1:2], turned[0:tok, 3:4], 0.0)
        high = blend.astype(jnp.bfloat16)
        bh[...] = high
        bl[...] = (blend - high.astype(jnp.float32)).astype(jnp.bfloat16)

    for n in range(3):
        stage_copy(n).start()
    for n in range(R // 128):
        piece = pl.ds(n * 128, 128)
        scale_at[piece, :] = jnp.broadcast_to(gain[0:1, piece], (128, 128)).T
    remote = 3 * len(others)
    for n in range(remote):
        cast(n)
        if n > 0:
            z_send(*tasks[n - 1][:2])
    route()
    z_send(*tasks[remote - 1][:2])
    for n in range(remote, len(tasks)):
        cast(n)
        if n == remote:
            for p in peers:
                t_copy(p, t).start()
    arr[slots(t), :] = xs[slots(t), :]

    rows_all = arr.shape[0]
    M = min(256, rows_all)

    def multiply(a, src, first):
        acc = (gacc, uacc)[a]
        deep = pl.ds(pl.multiple_of(src * R, R), R)

        @pl.loop(0, rows_all // M)
        def _(m):
            rows = pl.ds(pl.multiple_of(m * M, M), M)
            value = jnp.dot(arr[rows, deep], wins[a][deep, :], preferred_element_type=jnp.float32)
            if first:
                acc[rows, :] = value
            else:
                acc[rows, :] += value

    def activate():
        @pl.loop(0, rows_all // 64)
        def _(m):
            rows = pl.ds(pl.multiple_of(m * 64, 64), 64)
            v = gacc[rows, :]
            hid[rows, :] = (v / (1.0 + jnp.exp(-v)) * uacc[rows, :]).astype(jnp.bfloat16)

    def partial_out(src, half):
        cols = cols_of(src, half)

        @pl.loop(0, rows_all // M)
        def _(m):
            rows = pl.ds(pl.multiple_of(m * M, M), M)
            pbf[rows, cols] = jnp.dot(hid[rows, :], dw[:, cols], preferred_element_type=jnp.float32).astype(jnp.bfloat16)

        for p in peers:
            p_copy(src, half, p, t).start()
        ret[slots(t), cols] = pbf[slots(t), cols]

    def mix(src, half, own):
        cols = cols_of(src, half)
        for p in peers:
            p_copy(src, half, p, p).wait_recv()
        value = jnp.dot(bh[...], ret[:, cols], preferred_element_type=jnp.float32) + jnp.dot(
            bl[...], ret[:, cols], preferred_element_type=jnp.float32)
        if own:
            mown[:, pl.ds(pl.multiple_of(half * H, H), H)] = value
        else:
            msend[:, cols] = value.astype(jnp.bfloat16)
            m_copy(src, half, f).start()

    for p in peers:
        t_copy(p, p).wait_recv()
    for a in (0, 1):
        multiply(a, f, True)

    pending = []

    def submit(src, half, own):
        partial_out(src, half)
        pending.append((src, half, own))
        if len(pending) > 1:
            mix(*pending.pop(0))

    def finish(a, src):
        for q in range(pieces_of[a]):
            y_copy(a, src, 1 - g, q).wait_recv()
        if a < 2:
            multiply(a, src, False)
        else:
            offer(src, 1 - g)

    waiting, done = [], []

    def offer(src, half):
        waiting.append((src, half, False))
        if len(done) == 2 * len(others):
            while waiting:
                submit(*waiting.pop(0))

    def settle(a, src):
        finish(a, src)
        if a < 2:
            done.append(src)
            if len(done) == 2 * len(others):
                activate()
                submit(f, 0, True)
                submit(f, 1, True)

    items = [(a, others[k]) for a, k in order]
    last = None
    for a, src in items:
        for q in range(pieces_of[a]):
            z_recv(a, src, q).wait_recv()
            y_copy(a, src, g, q).start()
        if last is not None:
            settle(*last)
        if a == 2:
            offer(src, g)
        last = (a, src)
    settle(*last)
    for entry in pending:
        mix(*entry)
    total = mown[...]
    for p in others:
        for half in range(2):
            m_copy(p, half, p).wait_recv()
        total = total + mrecv[p].astype(jnp.float32)
    mo[...] = total.astype(jnp.bfloat16)

    for p in peers:
        t_copy(p, t).wait_send()
        for c in range(F):
            for half in range(2):
                p_copy(c, half, p, t).wait_send()
    for k, p in enumerate(others):
        for a in range(3):
            for q in range(pieces_of[a]):
                z_copy(a, k, p, f, q).wait_send()
                y_copy(a, p, g, q).wait_send()
        for half in range(2):
            m_copy(p, half, f).wait_send()


def exchange(F, T, gate, up, down, gain, tokens, routes, weight):
    span = -(-tokens.shape[0] // 128) * 128
    R, FF = gate.shape
    C, D, H = FF // F, F * R, R // 2
    Q = 4
    tok, S = tokens.shape[0], EXPERTS * CAP
    bf, f32 = jnp.bfloat16, jnp.float32
    any_spec, vm = pl.BlockSpec(memory_space=pl.ANY), pl.BlockSpec(memory_space=pltpu.VMEM)
    dma = pltpu.SemaphoreType.DMA
    return pl.pallas_call(
        functools.partial(exchange_kernel, F, T, R, C, Q),
        name="exchange",
        out_shape=(pltpu.VMEM((D, C), bf), pltpu.VMEM((D, C), bf),
                   pltpu.VMEM((C, D), bf), jax.ShapeDtypeStruct((tok, R), bf)),
        in_specs=[any_spec] * 3 + [vm] * 4,
        out_specs=(vm, vm, vm, vm),
        scratch_shapes=[
            pltpu.VMEM((128, span), f32), pltpu.VMEM((span, 128), f32), pltpu.VMEM((R, 128), f32),
            pltpu.VMEM((3, H, C), f32), pltpu.VMEM((3, C, H), f32),
            pltpu.VMEM((2, F - 1, H, C), bf), pltpu.VMEM((F - 1, C, H), bf),
            pltpu.VMEM((tok, D), bf), pltpu.VMEM((S, D), bf), pltpu.VMEM((tok, S), bf), pltpu.VMEM((tok, S), bf),
            pltpu.VMEM((S, D), bf),
            pltpu.VMEM((S, C), f32), pltpu.VMEM((S, C), f32), pltpu.VMEM((S, C), bf),
            pltpu.VMEM((S, D), bf), pltpu.VMEM((S, D), bf), pltpu.VMEM((tok, D), bf),
            pltpu.VMEM((tok, R), f32), pltpu.VMEM((F, tok, R), bf),
            dma((3, F, Q)), dma((3, F, Q)), dma((3, F, Q)), dma((3, F, Q)), dma((T,)), dma((T,)),
            dma((F, 2, T)), dma((F, 2, T)), dma((F, 2)), dma((F, 2)), dma((6,)),
        ],
        compiler_params=pltpu.CompilerParams(collective_id=0, has_side_effects=True, vmem_limit_bytes=42 * 1024 * 1024),
    )(gate, up, down, gain[None, :], tokens, routes.T, weight.T)


def fits(grp_count, fs_count, pieces, gate_train):
    rows, wide = gate_train.shape[1:]
    return (grp_count == 2 and fs_count == pieces and fs_count % 2 == 0
            and wide % (fs_count * 128) == 0 and rows % 256 == 0 and 4 <= 2 * fs_count <= 8)


def shards(tokens, routes, route_weight, norm_gain, gate_train, up_train, down_train):
    fs_count = lax.axis_size("fs")
    pieces = min(fs_count, 32)
    copies = fs_count // pieces
    if fits(lax.axis_size("grp"), fs_count, pieces, gate_train):
        gate_new, up_new, down_new, mixed = exchange(
            fs_count, lax.axis_size("tp"), gate_train[0], up_train[0], down_train[0],
            norm_gain, tokens, routes, route_weight,
        )
        return (gate_new[None], up_new[None], down_new[None], mixed)
    gain_column = norm_gain[:, None]
    gate_low = (gate_train[0] * gain_column).astype(jnp.bfloat16)
    up_low = (up_train[0] * gain_column).astype(jnp.bfloat16)
    down_low = down_train[0].astype(jnp.bfloat16)
    gate_wide = jnp.tile(gate_low, (1, copies))
    up_wide = jnp.tile(up_low, (1, copies))
    down_wide = jnp.tile(down_low, (copies, 1))
    gate_new, up_new = (
        lax.all_to_all(gate_wide, "fs", split_axis=1, concat_axis=0, tiled=True),
        lax.all_to_all(up_wide, "fs", split_axis=1, concat_axis=0, tiled=True),
    )
    down_new = lax.all_to_all(down_wide, "fs", split_axis=0, concat_axis=1, tiled=True)
    tok_float = tokens.astype(jnp.float32)
    normed = (
        tok_float * lax.rsqrt(jnp.mean(tok_float * tok_float, axis=-1, keepdims=True) + 1e-06)
    ).astype(jnp.bfloat16)
    chosen = routes.reshape(-1)
    chosen_hot = (chosen[:, None] == jnp.arange(EXPERTS, dtype=jnp.int32)[None, :]).astype(
        jnp.int32
    )
    before = jnp.cumsum(chosen_hot, axis=0) - chosen_hot
    slot_rank = jnp.sum(before * chosen_hot, axis=1)
    slot_index = (chosen * CAP + slot_rank).reshape(routes.shape)
    slot_range = jnp.arange(EXPERTS * CAP, dtype=jnp.int32)
    select_rows = jnp.any(slot_range[:, None, None] == slot_index[None, :, :], axis=-1).astype(
        jnp.bfloat16
    )
    outgoing = jnp.dot(select_rows, normed, preferred_element_type=jnp.float32).astype(jnp.bfloat16)
    outgoing = outgoing.reshape(EXPERTS, CAP, normed.shape[1])
    arrived = lax.all_to_all(outgoing, "tp", split_axis=0, concat_axis=0, tiled=True).reshape(
        EXPERTS * CAP, normed.shape[1]
    )
    slot_count = EXPERTS * CAP // copies
    copy_index = lax.axis_index("fs") // pieces
    my_rows = lax.dynamic_slice_in_dim(arrived, copy_index * slot_count, slot_count, 0)
    gated = jnp.dot(my_rows, gate_new, preferred_element_type=jnp.float32)
    lifted = jnp.dot(my_rows, up_new, preferred_element_type=jnp.float32)
    hidden = (jax.nn.silu(gated) * lifted).astype(jnp.bfloat16)
    partial_out = jnp.dot(hidden, down_new, preferred_element_type=jnp.float32)
    placed = jnp.zeros((EXPERTS * CAP, partial_out.shape[1]), jnp.float32)
    placed = lax.dynamic_update_slice_in_dim(placed, partial_out, copy_index * slot_count, 0)
    expert_out = lax.psum_scatter(placed, "fs", scatter_dimension=1, tiled=True).astype(
        jnp.bfloat16
    )
    returned = lax.all_to_all(
        expert_out.reshape(EXPERTS, CAP, expert_out.shape[1]),
        "tp",
        split_axis=0,
        concat_axis=0,
        tiled=True,
    )
    returned = returned.reshape(EXPERTS * CAP, expert_out.shape[1]).astype(jnp.float32)
    blend_weight = jnp.sum(
        jnp.where(
            slot_range[None, None, :] == slot_index[:, :, None], route_weight[:, :, None], 0.0
        ),
        axis=1,
    )
    mixed = jnp.dot(
        blend_weight, returned, precision=lax.Precision.HIGHEST, preferred_element_type=jnp.float32
    )
    return (gate_new[None], up_new[None], down_new[None], mixed.astype(jnp.bfloat16))


def solution(mesh):
    in_specs = (
        P(("grp", "tp"), None),
        P(("grp", "tp"), None),
        P(("grp", "tp"), None),
        P("fs"),
        P("tp", "fs", None),
        P("tp", "fs", None),
        P("tp", None, "fs"),
    )
    out_specs = (
        P(("grp", "tp"), None, "fs"),
        P(("grp", "tp"), None, "fs"),
        P(("grp", "tp"), "fs", None),
        P(("grp", "tp"), "fs"),
    )
    return jax.shard_map(shards, mesh=mesh, in_specs=in_specs, out_specs=out_specs, check_vma=False)
```

profile of v0, /device:TPU:9, one launch (start us, length us, event | category | flops | bytes accessed | tf_op | source)
XLA Modules:
  0.0 235.5 jit_solution(6881161125158670626)
XLA Ops:
  0.6 226.6 %exchange.1 = (bf16[2048,1408]{1,0:T(8,128)(2,1)S(1)}, bf16[2048,1408]{1,0:T(8,128)(2,1)S(1)}, bf16[1408,2048]{1,0:T(8,128)(2,1)S(1)}, bf16[192,512]{1,0:T(8,128)(2,1)}) custom-call(f32[512,5632]{1,0:T(8,128)} %bitcast.12, f32[512,5632]{1,0:T(8,128)} %bitcast.13, f32[5632,512]{1,0:T(8,128)} %bitcast.14, f32[1,512]{1,0:T(1,128)} %bitcast.15, ...), custom_call_target="tpu_custom_call" | custom-call | tf_op jit(solution)/shard_map/exchange/pallas_call | solution.py:311
  227.2 2.5 %copy.15 = bf16[1,2048,1408]{2,1,0:T(8,128)(2,1)} copy(bf16[1,2048,1408]{2,1,0:T(8,128)(2,1)S(1)} %bitcast.11) | data formatting | bytes 11534336
  229.7 2.5 %copy.16 = bf16[1,2048,1408]{2,1,0:T(8,128)(2,1)} copy(bf16[1,2048,1408]{2,1,0:T(8,128)(2,1)S(1)} %bitcast.10) | data formatting | bytes 11534336
  232.3 0.0 copy-start
  232.3 2.5 %copy.17 = bf16[1,1408,2048]{2,1,0:T(8,128)(2,1)} copy(bf16[1,1408,2048]{2,1,0:T(8,128)(2,1)S(1)} %bitcast.9) | data formatting | bytes 11534336
  234.8 0.0 copy-done
  234.8 0.7 copy.18
Async XLA Ops:
  232.3 2.5 %copy-start = (bf16[192,512]{1,0:T(8,128)(2,1)S(1)}, bf16[192,512]{1,0:T(8,128)(2,1)}, u32[]{:S(2)}) copy-start(bf16[192,512]{1,0:T(8,128)(2,1)} %get-tuple-element.23) | copy-start | bytes 589828
where the time goes:
time: 236 us; the launch traced here: 235 us
  Pallas kernels  227 us (96%)
  local copies, waits for them, and re-layouts  8.27 us (4%)
    pallas_call x1, Pallas kernels, exchange(): pl.pallas_call(functools.partial(exchange_kernel, F, T, R, C, Q), name='e...  227 us
    unnamed x6, local copies, waits for them, and re-layouts  8.27 us

commit v1 on v0

--- a/solution.py
+++ b/solution.py
@@ -11,19 +11,35 @@
 MESH = pl.DeviceIdType.MESH
 
 
-def exchange_kernel(F, T, R, C, Q, gt, ut, dt, gain, tokens, routes_t, weight_t, gw, uw, dw, mo,
+def exchange_kernel(F, T, R, C, Q, gt, ut, dt, gain, tokens, routes_t, weight_t, gw, uw, dw, mown, mrecv,
                     flat, turned, scale_at, wide, tall, sendw, sendt, normed, xs, bh, bl,
-                    arr, gacc, uacc, hid, pbf, ret, msend, mown, mrecv,
+                    arr, gacc, uacc, hid, pbf, ret, msend, shared,
                     zs, zr, ys, yr, ts, tr, ps, pr, ms, mr, loc):
     g, f, t = lax.axis_index("grp"), lax.axis_index("fs"), lax.axis_index("tp")
     H = R // 2
     wins = (gw, uw, dw)
-    pieces_of = (1, 1, Q)
-    half_f = F // 2
-    lo = lax.div(f, half_f)
+    low = 1 - lax.div(f, 2)
+    inner = lax.rem(lax.div(f + 1, 2), 2)
+    near = f + 1 - 2 * lax.rem(f, 2)
+    far_in = 1 + low
+    far_out = 3 * low
     peers = [lax.rem(t + d, T) for d in range(1, T)]
-    others = [lo * k + (1 - lo) * (F - 1 - k) for k in range(half_f)]
-    others += [lo * half_f + lax.rem(f - lo * half_f + 1 + j, half_f) for j in range(half_f - 1)]
+    others = [near, far_in, far_out]
+
+    def pick(if_inner, if_outer):
+        return inner * if_inner + (1 - inner) * if_outer
+
+    cross = pick(far_in, far_out)
+    targets = (
+        (pick(far_out, near), pick(near, far_in), pick(far_in, far_out)),
+        (near, far_in, far_out),
+        (near, pick(far_out, far_in), pick(far_in, far_out)),
+    )
+    sources = (
+        (pick(near, far_in), pick(far_out, near), pick(far_in, far_out)),
+        (near, far_out, far_in),
+        (near, far_out, far_in),
+    )
 
     barrier = pltpu.get_barrier_semaphore()
     for p in peers:
@@ -31,25 +47,27 @@
     for p in others:
         pl.semaphore_signal(barrier, inc=1, device_id={"fs": p}, device_id_type=MESH)
     pl.semaphore_signal(barrier, inc=1, device_id={"grp": 1 - g}, device_id_type=MESH)
-    pl.semaphore_wait(barrier, len(peers) + len(others) + 1)
 
     def cols_of(src, half):
         return pl.ds(pl.multiple_of(src * R + half * H, H), H)
 
+    def half_cols(half):
+        return pl.ds(pl.multiple_of(half * H, H), H)
+
     def part(a, src, half, q):
         if a < 2:
-            return wins[a].at[cols_of(src, half), :]
+            return wins[a].at[pl.ds(pl.multiple_of(src * R + half * H + q * (H // Q), H // Q), H // Q), :]
         return dw.at[pl.ds(q * (C // Q), C // Q), cols_of(src, half)]
 
-    def z_copy(a, k, tgt, src, q):
-        piece = sendw.at[a, k] if a < 2 else sendt.at[k, pl.ds(q * (C // Q), C // Q), :]
+    def z_copy(a, k, q):
+        piece = sendw.at[a, k, pl.ds(q * (H // Q), H // Q), :] if a < 2 else sendt.at[k, pl.ds(q * (C // Q), C // Q), :]
         return pltpu.make_async_remote_copy(
-            src_ref=piece, dst_ref=part(a, src, g, q), send_sem=zs.at[a, k, q], recv_sem=zr.at[a, src, q],
-            device_id={"fs": tgt}, device_id_type=MESH)
+            src_ref=piece, dst_ref=part(a, f, g, q), send_sem=zs.at[a, k, q], recv_sem=zr.at[a, f, q],
+            device_id={"fs": targets[a][k]}, device_id_type=MESH)
 
     def z_send(a, k):
-        for q in range(pieces_of[a]):
-            z_copy(a, k, others[k], f, q).start()
+        for q in range(Q):
+            z_copy(a, k, q).start()
 
     def z_recv(a, src, q):
         return pltpu.make_async_remote_copy(
@@ -76,40 +94,42 @@
             send_sem=ps.at[c, half, tgt], recv_sem=pr.at[c, half, src],
             device_id={"tp": tgt}, device_id_type=MESH)
 
-    def m_copy(tgt, half, src):
+    def m_copy(kind, block, half):
+        dst = shared.at[:, half_cols(half)] if kind == 2 else mrecv.at[kind, :, half_cols(half)]
         return pltpu.make_async_remote_copy(
-            src_ref=msend.at[:, cols_of(tgt, half)], dst_ref=mrecv.at[src, :, pl.ds(pl.multiple_of(half * H, H), H)],
-            send_sem=ms.at[tgt, half], recv_sem=mr.at[src, half],
-            device_id={"fs": tgt}, device_id_type=MESH)
-
-    if len(others) == 3:
-        order = [(0, 0), (0, 1), (0, 2), (1, 0), (1, 2), (2, 2), (1, 1), (2, 0), (2, 1)]
-    else:
-        order = [(a, k) for a in range(3) for k in range(len(others))]
-    tasks = [(a, k, g) for a, k in order]
+            src_ref=msend.at[:, cols_of(block, half)], dst_ref=dst,
+            send_sem=ms.at[kind, half], recv_sem=mr.at[kind, half],
+            device_id={"fs": cross if kind == 1 else near}, device_id_type=MESH)
+
+    tasks = [(a, k, g) for a in range(3) for k in range(3)]
     tasks += [(a, None, half) for a in range(3) for half in range(2)]
 
     def stage_copy(n):
         a, k, half = tasks[n]
-        tgt = f if k is None else others[k]
-        near, far = pl.ds(pl.multiple_of(half * H, H), H), pl.ds(pl.multiple_of(tgt * C, C), C)
+        tgt = f if k is None else targets[a][k]
+        rows, cols = half_cols(half), pl.ds(pl.multiple_of(tgt * C, C), C)
         if a < 2:
-            return pltpu.make_async_copy((gt, ut)[a].at[near, far], wide.at[n % 3], loc.at[n % 3])
-        return pltpu.make_async_copy(dt.at[far, near], tall.at[n % 3], loc.at[3 + n % 3])
+            return pltpu.make_async_copy((gt, ut)[a].at[rows, cols], wide.at[n % 3], loc.at[n % 3])
+        return pltpu.make_async_copy(dt.at[cols, rows], tall.at[n % 3], loc.at[3 + n % 3])
+
+    def cast_wide(n, begin, end):
+        a, k, half = tasks[n]
+
+        @pl.loop(begin // 32, end // 32)
+        def _(m):
+            rows = pl.ds(pl.multiple_of(m * 32, 32), 32)
+            scale = scale_at[pl.ds(pl.multiple_of(half * H + m * 32, 32), 32), 0:1]
+            value = (wide[n % 3, rows, :] * scale).astype(jnp.bfloat16)
+            if k is None:
+                wins[a][pl.ds(pl.multiple_of(f * R + half * H + m * 32, 32), 32), :] = value
+            else:
+                sendw[a, k, rows, :] = value
 
     def cast(n):
         a, k, half = tasks[n]
         stage_copy(n).wait()
         if a < 2:
-            @pl.loop(0, H // 32)
-            def _(m):
-                rows = pl.ds(pl.multiple_of(m * 32, 32), 32)
-                scale = scale_at[pl.ds(pl.multiple_of(half * H + m * 32, 32), 32), 0:1]
-                value = (wide[n % 3, rows, :] * scale).astype(jnp.bfloat16)
-                if k is None:
-                    wins[a][pl.ds(pl.multiple_of(f * R + half * H + m * 32, 32), 32), :] = value
-                else:
-                    sendw[a, k, rows, :] = value
+            cast_wide(n, 0, H)
         else:
             @pl.loop(0, C // 128)
             def _(m):
@@ -165,16 +185,34 @@
     for n in range(R // 128):
         piece = pl.ds(n * 128, 128)
         scale_at[piece, :] = jnp.broadcast_to(gain[0:1, piece], (128, 128)).T
-    remote = 3 * len(others)
-    for n in range(remote):
+    stage_copy(0).wait()
+    for q in range(Q):
+        cast_wide(0, q * (H // Q), (q + 1) * (H // Q))
+        if q == 0:
+            pl.semaphore_wait(barrier, len(peers) + len(others) + 1)
+        else:
+            z_copy(0, 0, q - 1).start()
+    stage_copy(3).start()
+    for n in range(1, 9):
         cast(n)
-        if n > 0:
-            z_send(*tasks[n - 1][:2])
+        a, k = tasks[n - 1][:2]
+        if n == 1:
+            z_copy(0, 0, Q - 1).start()
+        elif a == 2 and k > 0:
+            @pl.when(inner == 1)
+            def _():
+                z_send(a, k)
+        else:
+            z_send(a, k)
     route()
-    z_send(*tasks[remote - 1][:2])
-    for n in range(remote, len(tasks)):
+
+    @pl.when(inner == 1)
+    def _():
+        z_send(2, 2)
+
+    for n in range(9, len(tasks)):
         cast(n)
-        if n == remote:
+        if n == 9:
             for p in peers:
                 t_copy(p, t).start()
     arr[slots(t), :] = xs[slots(t), :]
@@ -214,89 +252,119 @@
             p_copy(src, half, p, t).start()
         ret[slots(t), cols] = pbf[slots(t), cols]
 
-    def mix(src, half, own):
+    def mix(src, half):
         cols = cols_of(src, half)
         for p in peers:
             p_copy(src, half, p, p).wait_recv()
-        value = jnp.dot(bh[...], ret[:, cols], preferred_element_type=jnp.float32) + jnp.dot(
+        return jnp.dot(bh[...], ret[:, cols], preferred_element_type=jnp.float32) + jnp.dot(
             bl[...], ret[:, cols], preferred_element_type=jnp.float32)
-        if own:
-            mown[:, pl.ds(pl.multiple_of(half * H, H), H)] = value
-        else:
+
+    def mix_own(half):
+        mown[:, half_cols(half)] = mix(f, half)
+
+    def mix_near(half):
+        msend[:, cols_of(near, half)] = mix(near, half).astype(jnp.bfloat16)
+        m_copy(0, near, half).start()
+
+    def mix_far(src, half, joins):
+        cols = cols_of(src, half)
+        value = mix(src, half)
+
+        @pl.when(joins == 1)
+        def _():
+            m_copy(2, src, half).wait_recv()
+            both = value + shared[:, half_cols(half)].astype(jnp.float32)
+            msend[:, cols] = both.astype(jnp.bfloat16)
+            m_copy(1, src, half).start()
+
+        @pl.when(joins == 0)
+        def _():
             msend[:, cols] = value.astype(jnp.bfloat16)
-            m_copy(src, half, f).start()
-
+            m_copy(2, src, half).start()
+
+    def arrive(a, src, middle=None):
+        for q in range(Q):
+            z_recv(a, src, q).wait_recv()
+            y_copy(a, src, g, q).start()
+            if q == 1 and middle is not None:
+                middle()
+
+    def settle(a, src):
+        for q in range(Q):
+            y_copy(a, src, 1 - g, q).wait_recv()
+        if a < 2:
+            multiply(a, src, False)
+
+    items = [(a, sources[a][k]) for a in range(2) for k in range(3)]
+    arrive(*items[0])
+    arrive(*items[1])
     for p in peers:
         t_copy(p, p).wait_recv()
     for a in (0, 1):
         multiply(a, f, True)
-
-    pending = []
-
-    def submit(src, half, own):
-        partial_out(src, half)
-        pending.append((src, half, own))
-        if len(pending) > 1:
-            mix(*pending.pop(0))
-
-    def finish(a, src):
-        for q in range(pieces_of[a]):
-            y_copy(a, src, 1 - g, q).wait_recv()
-        if a < 2:
-            multiply(a, src, False)
-        else:
-            offer(src, 1 - g)
-
-    waiting, done = [], []
-
-    def offer(src, half):
-        waiting.append((src, half, False))
-        if len(done) == 2 * len(others):
-            while waiting:
-                submit(*waiting.pop(0))
-
-    def settle(a, src):
-        finish(a, src)
-        if a < 2:
-            done.append(src)
-            if len(done) == 2 * len(others):
-                activate()
-                submit(f, 0, True)
-                submit(f, 1, True)
-
-    items = [(a, others[k]) for a, k in order]
-    last = None
-    for a, src in items:
-        for q in range(pieces_of[a]):
-            z_recv(a, src, q).wait_recv()
-            y_copy(a, src, g, q).start()
-        if last is not None:
-            settle(*last)
-        if a == 2:
-            offer(src, g)
-        last = (a, src)
-    settle(*last)
-    for entry in pending:
-        mix(*entry)
-    total = mown[...]
-    for p in others:
-        for half in range(2):
-            m_copy(p, half, p).wait_recv()
-        total = total + mrecv[p].astype(jnp.float32)
-    mo[...] = total.astype(jnp.bfloat16)
+    settle(*items[0])
+    for n in range(2, 6):
+        arrive(*items[n], middle=functools.partial(settle, *items[n - 1]))
+
+    @pl.when(inner == 0)
+    def _():
+        z_send(2, 1)
+        z_send(2, 2)
+
+    arrive(2, near)
+    settle(*items[5])
+    activate()
+    partial_out(f, 0)
+    partial_out(f, 1)
+    partial_out(near, g)
+    settle(2, near)
+    partial_out(near, 1 - g)
+    mix_own(0)
+    mix_own(1)
+    mix_near(g)
+    arrive(2, far_out, middle=functools.partial(mix_near, 1 - g))
+    partial_out(far_out, g)
+    settle(2, far_out)
+    partial_out(far_out, 1 - g)
+    mix_far(far_out, g, 1 - inner)
+    mix_far(far_out, 1 - g, 1 - inner)
+    arrive(2, far_in)
+    partial_out(far_in, g)
+    settle(2, far_in)
+    partial_out(far_in, 1 - g)
+    mix_far(far_in, g, inner)
+    mix_far(far_in, 1 - g, inner)
+    for half in range(2):
+        for kind in range(2):
+            m_copy(kind, near, half).wait_recv()
 
     for p in peers:
         t_copy(p, t).wait_send()
         for c in range(F):
             for half in range(2):
                 p_copy(c, half, p, t).wait_send()
-    for k, p in enumerate(others):
-        for a in range(3):
-            for q in range(pieces_of[a]):
-                z_copy(a, k, p, f, q).wait_send()
-                y_copy(a, p, g, q).wait_send()
-        for half in range(2):
-            m_copy(p, half, f).wait_send()
+    for a in range(3):
+        for k in range(3):
+            for q in range(Q):
+                z_copy(a, k, q).wait_send()
+                y_copy(a, others[k], g, q).wait_send()
+    for half in range(2):
+        for kind in range(3):
+            m_copy(kind, near, half).wait_send()
+
+
+def deliver_kernel(gw, uw, dw, mown, mrecv, go, uo, do, mo, total, sems):
+    copies = [pltpu.make_async_copy(a, b, sems.at[n]) for n, (a, b) in enumerate(((gw, go), (uw, uo), (dw, do)))]
+    for copy in copies:
+        copy.start()
+    value = mown[...]
+    for n in range(mrecv.shape[0]):
+        value = value + mrecv[n].astype(jnp.float32)
+    total[...] = value.astype(jnp.bfloat16)
+    last = pltpu.make_async_copy(total, mo, sems.at[len(copies)])
+    last.start()
+    for copy in copies + [last]:
+        copy.wait()
 
 
 def exchange(F, T, gate, up, down, gain, tokens, routes, weight):
@@ -308,13 +376,13 @@
     bf, f32 = jnp.bfloat16, jnp.float32
     any_spec, vm = pl.BlockSpec(memory_space=pl.ANY), pl.BlockSpec(memory_space=pltpu.VMEM)
     dma = pltpu.SemaphoreType.DMA
-    return pl.pallas_call(
+    held = pl.pallas_call(
         functools.partial(exchange_kernel, F, T, R, C, Q),
         name="exchange",
-        out_shape=(pltpu.VMEM((D, C), bf), pltpu.VMEM((D, C), bf),
-                   pltpu.VMEM((C, D), bf), jax.ShapeDtypeStruct((tok, R), bf)),
+        out_shape=(pltpu.VMEM((D, C), bf), pltpu.VMEM((D, C), bf), pltpu.VMEM((C, D), bf),
+                   pltpu.VMEM((tok, R), f32), pltpu.VMEM((2, tok, R), bf)),
         in_specs=[any_spec] * 3 + [vm] * 4,
-        out_specs=(vm, vm, vm, vm),
+        out_specs=(vm,) * 5,
         scratch_shapes=[
             pltpu.VMEM((128, span), f32), pltpu.VMEM((span, 128), f32), pltpu.VMEM((R, 128), f32),
             pltpu.VMEM((3, H, C), f32), pltpu.VMEM((3, C, H), f32),
@@ -322,19 +390,28 @@
             pltpu.VMEM((tok, D), bf), pltpu.VMEM((S, D), bf), pltpu.VMEM((tok, S), bf), pltpu.VMEM((tok, S), bf),
             pltpu.VMEM((S, D), bf),
             pltpu.VMEM((S, C), f32), pltpu.VMEM((S, C), f32), pltpu.VMEM((S, C), bf),
-            pltpu.VMEM((S, D), bf), pltpu.VMEM((S, D), bf), pltpu.VMEM((tok, D), bf),
-            pltpu.VMEM((tok, R), f32), pltpu.VMEM((F, tok, R), bf),
-            dma((3, F, Q)), dma((3, F, Q)), dma((3, F, Q)), dma((3, F, Q)), dma((T,)), dma((T,)),
-            dma((F, 2, T)), dma((F, 2, T)), dma((F, 2)), dma((F, 2)), dma((6,)),
+            pltpu.VMEM((S, D), bf), pltpu.VMEM((S, D), bf), pltpu.VMEM((tok, D), bf), pltpu.VMEM((tok, R), bf),
+            dma((3, F - 1, Q)), dma((3, F, Q)), dma((3, F, Q)), dma((3, F, Q)), dma((T,)), dma((T,)),
+            dma((F, 2, T)), dma((F, 2, T)), dma((3, 2)), dma((3, 2)), dma((6,)),
         ],
         compiler_params=pltpu.CompilerParams(collective_id=0, has_side_effects=True, vmem_limit_bytes=42 * 1024 * 1024),
     )(gate, up, down, gain[None, :], tokens, routes.T, weight.T)
+    return pl.pallas_call(
+        deliver_kernel,
+        name="deliver",
+        out_shape=(jax.ShapeDtypeStruct((D, C), bf), jax.ShapeDtypeStruct((D, C), bf),
+                   jax.ShapeDtypeStruct((C, D), bf), jax.ShapeDtypeStruct((tok, R), bf)),
+        in_specs=[vm] * 5,
+        out_specs=(pl.BlockSpec(memory_space=pltpu.HBM),) * 4,
+        scratch_shapes=[pltpu.VMEM((tok, R), bf), dma((4,))],
+        compiler_params=pltpu.CompilerParams(vmem_limit_bytes=4 * 1024 * 1024),
+    )(*[pltpu.with_memory_space_constraint(x, pltpu.VMEM) for x in held])
 
 
 def fits(grp_count, fs_count, pieces, gate_train):
     rows, wide = gate_train.shape[1:]
-    return (grp_count == 2 and fs_count == pieces and fs_count % 2 == 0
-            and wide % (fs_count * 128) == 0 and rows % 256 == 0 and 4 <= 2 * fs_count <= 8)
+    return (grp_count == 2 and fs_count == pieces and fs_count == 4
+            and wide % (fs_count * 128) == 0 and rows % 256 == 0)
 
 
 def shards(tokens, routes, route_weight, norm_gain, gate_train, up_train, down_train):

time: 236 us -> 229 us (0.970)
  local copies, waits for them, and re-layouts: 8.27 us -> 0 us
    unnamed x6 -> x0, local copies, waits for them, and re-layouts: 8.27 us -> none
    pallas_call x0 -> x1, Pallas kernels: none -> 6.2 us  [exchange(): pl.pallas_call(deliver_kernel, name='deliver', out_shape=(jax.ShapeDtypeS...]
    pallas_call x1, Pallas kernels: 227 us -> 222 us  [exchange(): pl.pallas_call(functools.partial(exchange_kernel, F, T, R, C, Q), name='e...]
where the time goes in v1:
time: 229 us
  Pallas kernels  228 us (100%)
    pallas_call x1, Pallas kernels, exchange(): pl.pallas_call(functools.partial(exchange_kernel, F, T, R, C, Q), name='e...  222 us
    pallas_call x1, Pallas kernels, exchange(): pl.pallas_call(deliver_kernel, name='deliver', out_shape=(jax.ShapeDtypeS...  6.2 us

profile of v1, /device:TPU:9, one launch (start us, length us, event | category | flops | bytes accessed | tf_op | source)
XLA Modules:
  0.0 228.7 jit_solution(9444087238030944056)
XLA Ops:
  0.6 221.9 %exchange.1 = (bf16[2048,1408]{1,0:T(8,128)(2,1)S(1)}, bf16[2048,1408]{1,0:T(8,128)(2,1)S(1)}, bf16[1408,2048]{1,0:T(8,128)(2,1)S(1)}, f32[192,512]{1,0:T(8,128)S(1)}, bf16[2,192,512]{2,1,0:T(8,128)(2,1)S(1)}) custom-call(f32[512,5632]{1,0:T(8,128)} %bitcast.9, f32[512,5632]{1,0:T(8,128)} %bitcast.10, f32[5632,512]{1,0:T(8,128)} %bitcast.11, ...), custom_call_target="tpu_custom_call" | custom-call | tf_op jit(solution)/shard_map/exchange/pallas_call | solution.py:379
  222.5 6.2 %deliver.1 = (bf16[2048,1408]{1,0:T(8,128)(2,1)}, bf16[2048,1408]{1,0:T(8,128)(2,1)}, bf16[1408,2048]{1,0:T(8,128)(2,1)}, bf16[192,512]{1,0:T(8,128)(2,1)}) custom-call(bf16[2048,1408]{1,0:T(8,128)(2,1)S(1)} %get-tuple-element.13.gw, bf16[2048,1408]{1,0:T(8,128)(2,1)S(1)} %get-tuple-element.14.uw, bf16[1408,2048]{1,0:T(8,128)(2,1)S(1)} %get-tuple-element.15.dw, ...), custom_call_target="tpu_custom_call" | custom-call | tf_op jit(solution)/shard_map/deliver/pallas_call | solution.py:399

commit v2 on v1

--- a/solution.py
+++ b/solution.py
@@ -11,10 +11,10 @@
 MESH = pl.DeviceIdType.MESH
 
 
-def exchange_kernel(F, T, R, C, Q, gt, ut, dt, gain, tokens, routes_t, weight_t, gw, uw, dw, mown, mrecv,
-                    flat, turned, scale_at, wide, tall, sendw, sendt, normed, xs, bh, bl,
+def exchange_kernel(F, T, R, C, Q, NEAR, OUT, FINE, gt, ut, dt, gain_at, tokens_at, routes_at, weight_at, gw, uw, dw, mown, mrecv,
+                    gain, tokens, routes_t, weight_t, flat, turned, scale_at, wide, tall, sendw, sendt, normed, xs, bh, bl,
                     arr, gacc, uacc, hid, pbf, ret, msend, shared,
-                    zs, zr, ys, yr, ts, tr, ps, pr, ms, mr, loc):
+                    zs, zr, zt, ys, yr, yt, ts, ps, pr, ms, mr, loc, first):
     g, f, t = lax.axis_index("grp"), lax.axis_index("fs"), lax.axis_index("tp")
     H = R // 2
     wins = (gw, uw, dw)
@@ -25,20 +25,23 @@
     far_out = 3 * low
     peers = [lax.rem(t + d, T) for d in range(1, T)]
     others = [near, far_in, far_out]
+    far = [far_out, far_in]
 
     def pick(if_inner, if_outer):
         return inner * if_inner + (1 - inner) * if_outer
 
-    cross = pick(far_in, far_out)
     targets = (
-        (pick(far_out, near), pick(near, far_in), pick(far_in, far_out)),
+        (pick(far_out, near), far_in, pick(near, far_out)),
         (near, far_in, far_out),
         (near, pick(far_out, far_in), pick(far_in, far_out)),
     )
-    sources = (
-        (pick(near, far_in), pick(far_out, near), pick(far_in, far_out)),
-        (near, far_out, far_in),
-        (near, far_out, far_in),
+    places = (
+        (pick(2, 0), pick(2, 1), pick(0, 1)),
+        (0, pick(2, 1), pick(2, 1)),
+    )
+    items = (
+        (0, pick(near, far_in), pick(0, 2)), (0, pick(far_in, near), pick(2, 0)), (1, near, 0),
+        (0, far_out, 1), (1, pick(far_in, far_out), pick(2, 1)), (1, pick(far_out, far_in), pick(1, 2)),
     )
 
     barrier = pltpu.get_barrier_semaphore()
@@ -54,52 +57,94 @@
     def half_cols(half):
         return pl.ds(pl.multiple_of(half * H, H), H)
 
-    def part(a, src, half, q):
+    W = H // 2
+    WIDE = [(n * (H // Q), H // Q, 0, C) for n in range(Q)]
+    TALL = [[(n * (C // m), C // m, 0, H) for n in range(m)] for m in (NEAR, OUT)]
+    TALL.append([(n * (C // FINE), C // FINE, m * W, W) for m in range(2) for n in range(FINE)])
+    BASE = [0, len(TALL[0]), len(TALL[0]) + len(TALL[1])]
+
+    def part(a, src, half, piece):
+        row, rows, col, cols = piece
         if a < 2:
-            return wins[a].at[pl.ds(pl.multiple_of(src * R + half * H + q * (H // Q), H // Q), H // Q), :]
-        return dw.at[pl.ds(q * (C // Q), C // Q), cols_of(src, half)]
-
-    def z_copy(a, k, q):
-        piece = sendw.at[a, k, pl.ds(q * (H // Q), H // Q), :] if a < 2 else sendt.at[k, pl.ds(q * (C // Q), C // Q), :]
-        return pltpu.make_async_remote_copy(
-            src_ref=piece, dst_ref=part(a, f, g, q), send_sem=zs.at[a, k, q], recv_sem=zr.at[a, f, q],
+            return wins[a].at[pl.ds(pl.multiple_of(src * R + half * H + row, rows), rows), :]
+        return dw.at[pl.ds(row, rows), pl.ds(pl.multiple_of(src * R + half * H + col, W), cols)]
+
+    def z_copy(a, k, piece, sem):
+        row, rows, col, cols = piece
+        held = sendw.at[a, k, pl.ds(row, rows), :] if a < 2 else sendt.at[k, pl.ds(row, rows), pl.ds(col, cols)]
+        return pltpu.make_async_remote_copy(
+            src_ref=held, dst_ref=part(a, f, g, piece), send_sem=zs.at[min(a, 2) // 2], recv_sem=sem,
             device_id={"fs": targets[a][k]}, device_id_type=MESH)
 
-    def z_send(a, k):
-        for q in range(Q):
-            z_copy(a, k, q).start()
-
-    def z_recv(a, src, q):
-        return pltpu.make_async_remote_copy(
-            src_ref=part(a, src, g, q), dst_ref=part(a, src, g, q), send_sem=zs.at[a, 0, q],
-            recv_sem=zr.at[a, src, q], device_id={"fs": src}, device_id_type=MESH)
-
-    def y_copy(a, src, half, q):
-        return pltpu.make_async_remote_copy(
-            src_ref=part(a, src, half, q), dst_ref=part(a, src, half, q), send_sem=ys.at[a, src, q],
-            recv_sem=yr.at[a, src, q], device_id={"grp": 1 - g}, device_id_type=MESH)
+    def z_send(a, k, place=None):
+        if a < 2:
+            for q, piece in enumerate(WIDE):
+                z_copy(a, k, piece, zr.at[a, places[a][k], q]).start()
+        else:
+            for q, piece in enumerate(TALL[place]):
+                z_copy(a, k, piece, zt.at[BASE[place] + q]).start()
+
+    def z_recv(a, src, piece, sem):
+        here = part(a, src, g, piece)
+        return pltpu.make_async_remote_copy(
+            src_ref=here, dst_ref=here, send_sem=zs.at[min(a, 2) // 2], recv_sem=sem,
+            device_id={"fs": src}, device_id_type=MESH)
+
+    def y_copy(a, src, half, piece, sem):
+        here = part(a, src, half, piece)
+        return pltpu.make_async_remote_copy(
+            src_ref=here, dst_ref=here, send_sem=ys.at[a], recv_sem=sem,
+            device_id={"grp": 1 - g}, device_id_type=MESH)
+
+    def sent(ref, sem):
+        pltpu.make_async_remote_copy(
+            src_ref=ref, dst_ref=ref, send_sem=sem, recv_sem=sem,
+            device_id={"fs": near}, device_id_type=MESH).wait_send()
+
+    def received(ref, sem):
+        pltpu.make_async_remote_copy(
+            src_ref=ref, dst_ref=ref, send_sem=sem, recv_sem=sem,
+            device_id={"fs": near}, device_id_type=MESH).wait_recv()
 
     def slots(q):
         return pl.ds(pl.multiple_of(q * CAP, CAP), CAP)
 
     def t_copy(tgt, src):
         return pltpu.make_async_remote_copy(
-            src_ref=xs.at[slots(tgt), :], dst_ref=arr.at[slots(src), :], send_sem=ts.at[tgt], recv_sem=tr.at[src],
+            src_ref=xs.at[slots(tgt), :], dst_ref=arr.at[slots(src), :], send_sem=ts.at[0], recv_sem=ts.at[1],
             device_id={"tp": tgt}, device_id_type=MESH)
 
-    def p_copy(c, half, tgt, src):
-        cols = cols_of(c, half)
+    def unit(half, chunk):
+        if chunk is None:
+            return half_cols(half)
+        return pl.ds(pl.multiple_of(half * H + chunk * W, W), W)
+
+    def unit_of(c, half, chunk):
+        if chunk is None:
+            return cols_of(c, half)
+        return pl.ds(pl.multiple_of(c * R + half * H + chunk * W, W), W)
+
+    def p_copy(c, kind, half, chunk, tgt, src):
+        cols = unit_of(c, half, chunk)
         return pltpu.make_async_remote_copy(
             src_ref=pbf.at[slots(tgt), cols], dst_ref=ret.at[slots(src), cols],
-            send_sem=ps.at[c, half, tgt], recv_sem=pr.at[c, half, src],
+            send_sem=ps.at[0], recv_sem=pr.at[kind + (chunk or 0), half],
             device_id={"tp": tgt}, device_id_type=MESH)
 
-    def m_copy(kind, block, half):
-        dst = shared.at[:, half_cols(half)] if kind == 2 else mrecv.at[kind, :, half_cols(half)]
-        return pltpu.make_async_remote_copy(
-            src_ref=msend.at[:, cols_of(block, half)], dst_ref=dst,
-            send_sem=ms.at[kind, half], recv_sem=mr.at[kind, half],
-            device_id={"fs": cross if kind == 1 else near}, device_id_type=MESH)
+    def near_copy(half):
+        return pltpu.make_async_remote_copy(
+            src_ref=msend.at[:, cols_of(near, half)], dst_ref=mrecv.at[0, :, half_cols(half)],
+            send_sem=ms.at[0], recv_sem=mr.at[0], device_id={"fs": near}, device_id_type=MESH)
+
+    def share_copy(n, half):
+        return pltpu.make_async_remote_copy(
+            src_ref=msend.at[:, cols_of(far[n], half)], dst_ref=shared.at[n, :, half_cols(half)],
+            send_sem=ms.at[1 + n], recv_sem=mr.at[2 + n], device_id={"fs": near}, device_id_type=MESH)
+
+    def cross_copy(n, half, chunk):
+        return pltpu.make_async_remote_copy(
+            src_ref=msend.at[:, unit_of(far[n], half, chunk)], dst_ref=mrecv.at[1, :, unit(half, chunk)],
+            send_sem=ms.at[1 + n], recv_sem=mr.at[1], device_id={"fs": far[n]}, device_id_type=MESH)
 
     tasks = [(a, k, g) for a in range(3) for k in range(3)]
     tasks += [(a, None, half) for a in range(3) for half in range(2)]
@@ -180,35 +225,57 @@
         bh[...] = high
         bl[...] = (blend - high.astype(jnp.float32)).astype(jnp.bfloat16)
 
-    for n in range(3):
+    def first_copy(q):
+        rows = pl.ds(pl.multiple_of(g * H + q * (H // Q), H // Q), H // Q)
+        cols = pl.ds(pl.multiple_of(targets[0][0] * C, C), C)
+        return pltpu.make_async_copy(gt.at[rows, cols], wide.at[0, pl.ds(q * (H // Q), H // Q), :], first.at[q])
+
+    small = [pltpu.make_async_copy(a, b, first.at[Q + n]) for n, (a, b) in enumerate(
+        ((gain_at, gain), (tokens_at, tokens), (routes_at, routes_t), (weight_at, weight_t)))]
+    small[0].start()
+    for q in range(Q):
+        first_copy(q).start()
+    for n in range(1, 3):
         stage_copy(n).start()
+    for copy in small[1:]:
+        copy.start()
+    small[0].wait()
     for n in range(R // 128):
         piece = pl.ds(n * 128, 128)
         scale_at[piece, :] = jnp.broadcast_to(gain[0:1, piece], (128, 128)).T
-    stage_copy(0).wait()
     for q in range(Q):
+        first_copy(q).wait()
         cast_wide(0, q * (H // Q), (q + 1) * (H // Q))
         if q == 0:
             pl.semaphore_wait(barrier, len(peers) + len(others) + 1)
         else:
-            z_copy(0, 0, q - 1).start()
+            z_copy(0, 0, WIDE[q - 1], zr.at[0, places[0][0], q - 1]).start()
     stage_copy(3).start()
     for n in range(1, 9):
         cast(n)
         a, k = tasks[n - 1][:2]
         if n == 1:
-            z_copy(0, 0, Q - 1).start()
-        elif a == 2 and k > 0:
+            z_copy(0, 0, WIDE[Q - 1], zr.at[0, places[0][0], Q - 1]).start()
+        elif n < 8:
             @pl.when(inner == 1)
             def _():
-                z_send(a, k)
+                z_send(a, k, 0)
         else:
-            z_send(a, k)
+            @pl.when(inner == 1)
+            def _():
+                z_send(2, 1, 2)
+
+            @pl.when(inner == 0)
+            def _():
+                for pair in ((1, 0), (2, 0), (0, 1), (0, 2), (1, 1), (1, 2)):
+                    z_send(*pair, 0)
+    for copy in small[1:]:
+        copy.wait()
     route()
 
     @pl.when(inner == 1)
     def _():
-        z_send(2, 2)
+        z_send(2, 2, 2)
 
     for n in range(9, len(tasks)):
         cast(n)
@@ -240,8 +307,8 @@
             v = gacc[rows, :]
             hid[rows, :] = (v / (1.0 + jnp.exp(-v)) * uacc[rows, :]).astype(jnp.bfloat16)
 
-    def partial_out(src, half):
-        cols = cols_of(src, half)
+    def partial_out(c, kind, half, chunk=None):
+        cols = unit_of(c, half, chunk)
 
         @pl.loop(0, rows_all // M)
         def _(m):
@@ -249,108 +316,132 @@
             pbf[rows, cols] = jnp.dot(hid[rows, :], dw[:, cols], preferred_element_type=jnp.float32).astype(jnp.bfloat16)
 
         for p in peers:
-            p_copy(src, half, p, t).start()
+            p_copy(c, kind, half, chunk, p, t).start()
         ret[slots(t), cols] = pbf[slots(t), cols]
 
-    def mix(src, half):
-        cols = cols_of(src, half)
-        for p in peers:
-            p_copy(src, half, p, p).wait_recv()
+    def mix(c, kind, half, chunk=None):
+        cols = unit_of(c, half, chunk)
+        received(ret.at[pl.ds(0, len(peers) * CAP), cols], pr.at[kind + (chunk or 0), half])
         return jnp.dot(bh[...], ret[:, cols], preferred_element_type=jnp.float32) + jnp.dot(
             bl[...], ret[:, cols], preferred_element_type=jnp.float32)
 
     def mix_own(half):
-        mown[:, half_cols(half)] = mix(f, half)
+        mown[:, half_cols(half)] = mix(f, 0, half)
 
     def mix_near(half):
-        msend[:, cols_of(near, half)] = mix(near, half).astype(jnp.bfloat16)
-        m_copy(0, near, half).start()
-
-    def mix_far(src, half, joins):
-        cols = cols_of(src, half)
-        value = mix(src, half)
-
-        @pl.when(joins == 1)
-        def _():
-            m_copy(2, src, half).wait_recv()
-            both = value + shared[:, half_cols(half)].astype(jnp.float32)
-            msend[:, cols] = both.astype(jnp.bfloat16)
-            m_copy(1, src, half).start()
-
-        @pl.when(joins == 0)
-        def _():
-            msend[:, cols] = value.astype(jnp.bfloat16)
-            m_copy(2, src, half).start()
-
-    def arrive(a, src, middle=None):
-        for q in range(Q):
-            z_recv(a, src, q).wait_recv()
-            y_copy(a, src, g, q).start()
-            if q == 1 and middle is not None:
-                middle()
-
-    def settle(a, src):
-        for q in range(Q):
-            y_copy(a, src, 1 - g, q).wait_recv()
+        msend[:, cols_of(near, half)] = mix(near, 1, half).astype(jnp.bfloat16)
+        near_copy(half).start()
+
+    def join(n, half, chunk=None):
+        cols = unit_of(far[n], half, chunk)
+        both = mix(far[n], 2 + n, half, chunk) + shared[n, :, unit(half, chunk)].astype(jnp.float32)
+        msend[:, cols] = both.astype(jnp.bfloat16)
+        cross_copy(n, half, chunk).start()
+
+    def share(n, half):
+        msend[:, cols_of(far[n], half)] = mix(far[n], 2 + n, half).astype(jnp.bfloat16)
+        share_copy(n, half).start()
+
+    def stream(a, place):
         if a < 2:
-            multiply(a, src, False)
-
-    items = [(a, sources[a][k]) for a in range(2) for k in range(3)]
-    arrive(*items[0])
-    arrive(*items[1])
-    for p in peers:
-        t_copy(p, p).wait_recv()
+            return [(piece, zr.at[a, place, q], yr.at[a, place, q]) for q, piece in enumerate(WIDE)]
+        return [(piece, zt.at[BASE[place] + q], yt.at[BASE[place] + q]) for q, piece in enumerate(TALL[place])]
+
+    def forward(a, src, place, begin, end):
+        for piece, z, y in stream(a, place)[begin:end]:
+            z_recv(a, src, piece, z).wait_recv()
+            y_copy(a, src, g, piece, y).start()
+
+    def landed(a, src, place, begin=0, end=None):
+        for piece, _, y in stream(a, place)[begin:end]:
+            y_copy(a, src, 1 - g, piece, y).wait_recv()
+
+    def settle(a, src, place):
+        landed(a, src, place)
+        multiply(a, src, False)
+
+    half_way = Q // 2
+    forward(*items[0], 0, Q)
+    forward(*items[1], 0, Q)
+    received(xs.at[pl.ds(0, len(peers) * CAP), :], ts.at[1])
     for a in (0, 1):
         multiply(a, f, True)
-    settle(*items[0])
     for n in range(2, 6):
-        arrive(*items[n], middle=functools.partial(settle, *items[n - 1]))
+        forward(*items[n], 0, half_way)
+        settle(*items[n - 2])
+        forward(*items[n], half_way, Q)
+    settle(*items[4])
 
     @pl.when(inner == 0)
     def _():
-        z_send(2, 1)
-        z_send(2, 2)
-
-    arrive(2, near)
+        z_send(2, 1, 1)
+        z_send(2, 2, 1)
+
+    forward(2, near, 0, 0, NEAR)
     settle(*items[5])
     activate()
-    partial_out(f, 0)
-    partial_out(f, 1)
-    partial_out(near, g)
-    settle(2, near)
-    partial_out(near, 1 - g)
+    partial_out(f, 0, 0)
+    partial_out(f, 0, 1)
+    partial_out(near, 1, g)
+    landed(2, near, 0)
+    partial_out(near, 1, 1 - g)
     mix_own(0)
     mix_own(1)
     mix_near(g)
-    arrive(2, far_out, middle=functools.partial(mix_near, 1 - g))
-    partial_out(far_out, g)
-    settle(2, far_out)
-    partial_out(far_out, 1 - g)
-    mix_far(far_out, g, 1 - inner)
-    mix_far(far_out, 1 - g, 1 - inner)
-    arrive(2, far_in)
-    partial_out(far_in, g)
-    settle(2, far_in)
-    partial_out(far_in, 1 - g)
-    mix_far(far_in, g, inner)
-    mix_far(far_in, 1 - g, inner)
-    for half in range(2):
-        for kind in range(2):
-            m_copy(kind, near, half).wait_recv()
-
-    for p in peers:
-        t_copy(p, t).wait_send()
-        for c in range(F):
-            for half in range(2):
-                p_copy(c, half, p, t).wait_send()
+    forward(2, far_out, 1, 0, 1)
+    mix_near(1 - g)
+    forward(2, far_out, 1, 1, OUT)
+    partial_out(far_out, 2, g)
+
+    def forward_in(begin, end):
+        forward(2, far_in, 2, begin, end)
+
+    @pl.when(inner == 0)
+    def _():
+        forward_in(0, FINE)
+        landed(2, far_out, 1)
+        partial_out(far_out, 2, 1 - g)
+        forward_in(FINE, 2 * FINE)
+        share(0, g)
+        share(0, 1 - g)
+        partial_out(far_in, 3, g)
+        landed(2, far_in, 2)
+        partial_out(far_in, 3, 1 - g)
+        share(1, g)
+        share(1, 1 - g)
+
+    @pl.when(inner == 1)
+    def _():
+        landed(2, far_out, 1)
+        partial_out(far_out, 2, 1 - g)
+        forward_in(0, FINE)
+        partial_out(far_in, 3, g, 0)
+        forward_in(FINE, FINE + 1)
+        landed(2, far_in, 2, 0, FINE)
+        partial_out(far_in, 3, 1 - g, 0)
+        forward_in(FINE + 1, 2 * FINE)
+        partial_out(far_in, 3, g, 1)
+        received(shared.at[0], mr.at[2])
+        join(0, g)
+        join(0, 1 - g)
+        received(shared.at[1], mr.at[3])
+        join(1, g, 0)
+        join(1, 1 - g, 0)
+        landed(2, far_in, 2, FINE, 2 * FINE)
+        partial_out(far_in, 3, 1 - g, 1)
+        join(1, g, 1)
+        join(1, 1 - g, 1)
+
+    sent(xs.at[pl.ds(0, len(peers) * CAP), :], ts.at[0])
+    sent(sendw, zs.at[0])
+    sent(sendt, zs.at[1])
     for a in range(3):
-        for k in range(3):
-            for q in range(Q):
-                z_copy(a, k, q).wait_send()
-                y_copy(a, others[k], g, q).wait_send()
-    for half in range(2):
-        for kind in range(3):
-            m_copy(kind, near, half).wait_send()
+        sent(sendw.at[a] if a < 2 else sendt, ys.at[a])
+    sent(pbf.at[pl.ds(0, len(peers) * CAP), :], ps.at[0])
+    received(mrecv.at[0], mr.at[0])
+    received(mrecv.at[1], mr.at[1])
+    for n in range(3):
+        sent(msend.at[:, pl.ds(0, R)], ms.at[n])
 
 
 def deliver_kernel(gw, uw, dw, mown, mrecv, go, uo, do, mo, total, sems):
@@ -371,28 +462,29 @@
     span = -(-tokens.shape[0] // 128) * 128
     R, FF = gate.shape
     C, D, H = FF // F, F * R, R // 2
-    Q = 4
+    Q, NEAR, OUT, FINE = 4, 2, 4, 4
     tok, S = tokens.shape[0], EXPERTS * CAP
     bf, f32 = jnp.bfloat16, jnp.float32
     any_spec, vm = pl.BlockSpec(memory_space=pl.ANY), pl.BlockSpec(memory_space=pltpu.VMEM)
     dma = pltpu.SemaphoreType.DMA
     held = pl.pallas_call(
-        functools.partial(exchange_kernel, F, T, R, C, Q),
+        functools.partial(exchange_kernel, F, T, R, C, Q, NEAR, OUT, FINE),
         name="exchange",
         out_shape=(pltpu.VMEM((D, C), bf), pltpu.VMEM((D, C), bf), pltpu.VMEM((C, D), bf),
                    pltpu.VMEM((tok, R), f32), pltpu.VMEM((2, tok, R), bf)),
-        in_specs=[any_spec] * 3 + [vm] * 4,
+        in_specs=[any_spec] * 7,
         out_specs=(vm,) * 5,
         scratch_shapes=[
-            pltpu.VMEM((128, span), f32), pltpu.VMEM((span, 128), f32), pltpu.VMEM((R, 128), f32),
+            pltpu.VMEM((1, R), f32), pltpu.VMEM((tok, D), bf), pltpu.VMEM((routes.shape[1], tok), jnp.int32),
+            pltpu.VMEM((routes.shape[1], tok), f32), pltpu.VMEM((128, span), f32), pltpu.VMEM((span, 128), f32), pltpu.VMEM((R, 128), f32),
             pltpu.VMEM((3, H, C), f32), pltpu.VMEM((3, C, H), f32),
             pltpu.VMEM((2, F - 1, H, C), bf), pltpu.VMEM((F - 1, C, H), bf),
             pltpu.VMEM((tok, D), bf), pltpu.VMEM((S, D), bf), pltpu.VMEM((tok, S), bf), pltpu.VMEM((tok, S), bf),
             pltpu.VMEM((S, D), bf),
             pltpu.VMEM((S, C), f32), pltpu.VMEM((S, C), f32), pltpu.VMEM((S, C), bf),
-            pltpu.VMEM((S, D), bf), pltpu.VMEM((S, D), bf), pltpu.VMEM((tok, D), bf), pltpu.VMEM((tok, R), bf),
-            dma((3, F - 1, Q)), dma((3, F, Q)), dma((3, F, Q)), dma((3, F, Q)), dma((T,)), dma((T,)),
-            dma((F, 2, T)), dma((F, 2, T)), dma((3, 2)), dma((3, 2)), dma((6,)),
+            pltpu.VMEM((S, D), bf), pltpu.VMEM((S, D), bf), pltpu.VMEM((tok, D), bf), pltpu.VMEM((2, tok, R), bf),
+            dma((2,)), dma((2, F - 1, Q)), dma((NEAR + OUT + 2 * FINE,)), dma((3,)), dma((2, F - 1, Q)), dma((NEAR + OUT + 2 * FINE,)), dma((2,)),
+            dma((1,)), dma((5, 2)), dma((3,)), dma((4,)), dma((6,)), dma((Q + 4,)),
         ],
         compiler_params=pltpu.CompilerParams(collective_id=0, has_side_effects=True, vmem_limit_bytes=42 * 1024 * 1024),
     )(gate, up, down, gain[None, :], tokens, routes.T, weight.T)

time: 229 us -> 210 us (0.917)
  Pallas kernels: 228 us -> 209 us
    pallas_call x1, Pallas kernels: 222 us -> 203 us  [exchange(): pl.pallas_call(functools.partial(exchange_kernel, F, T, R, C, Q, NEAR, OU...]
where the time goes in v2:
time: 210 us
  Pallas kernels  209 us (100%)
    pallas_call x1, Pallas kernels, exchange(): pl.pallas_call(functools.partial(exchange_kernel, F, T, R, C, Q, NEAR, OU...  203 us
    pallas_call x1, Pallas kernels, exchange(): pl.pallas_call(deliver_kernel, name='deliver', out_shape=(jax.ShapeDtypeS...  6.2 us

profile of v2, /device:TPU:9, one launch (start us, length us, event | category | flops | bytes accessed | tf_op | source)
XLA Modules:
  0.0 209.9 jit_solution(16996099051500510488)
XLA Ops:
  0.6 202.9 %exchange.1 = (bf16[2048,1408]{1,0:T(8,128)(2,1)S(1)}, bf16[2048,1408]{1,0:T(8,128)(2,1)S(1)}, bf16[1408,2048]{1,0:T(8,128)(2,1)S(1)}, f32[192,512]{1,0:T(8,128)S(1)}, bf16[2,192,512]{2,1,0:T(8,128)(2,1)S(1)}) custom-call(f32[512,5632]{1,0:T(8,128)} %bitcast.9, f32[512,5632]{1,0:T(8,128)} %bitcast.10, f32[5632,512]{1,0:T(8,128)} %bitcast.11, ...), custom_call_target="tpu_custom_call" | custom-call | tf_op jit(solution)/shard_map/exchange/pallas_call | solution.py:470
  203.6 6.2 %deliver.1 = (bf16[2048,1408]{1,0:T(8,128)(2,1)}, bf16[2048,1408]{1,0:T(8,128)(2,1)}, bf16[1408,2048]{1,0:T(8,128)(2,1)}, bf16[192,512]{1,0:T(8,128)(2,1)}) custom-call(bf16[2048,1408]{1,0:T(8,128)(2,1)S(1)} %get-tuple-element.13.gw, bf16[2048,1408]{1,0:T(8,128)(2,1)S(1)} %get-tuple-element.14.uw, bf16[1408,2048]{1,0:T(8,128)(2,1)S(1)} %get-tuple-element.15.dw, ...), custom_call_target="tpu_custom_call" | custom-call | tf_op jit(solution)/shard_map/deliver/pallas_call | solution.py:491

commit v3 on v2

--- a/solution.py
+++ b/solution.py
@@ -13,8 +13,8 @@
 
 def exchange_kernel(F, T, R, C, Q, NEAR, OUT, FINE, gt, ut, dt, gain_at, tokens_at, routes_at, weight_at, gw, uw, dw, mown, mrecv,
                     gain, tokens, routes_t, weight_t, flat, turned, scale_at, wide, tall, sendw, sendt, normed, xs, bh, bl,
-                    arr, gacc, uacc, hid, pbf, ret, msend, shared,
-                    zs, zr, zt, ys, yr, yt, ts, ps, pr, ms, mr, loc, first):
+                    early, arr, gacc, uacc, hid, pbf, ret, msend, shared,
+                    zs, zr, zt, ys, yr, yt, ts, ps, pr, ms, mr, loc):
     g, f, t = lax.axis_index("grp"), lax.axis_index("fs"), lax.axis_index("tp")
     H = R // 2
     wins = (gw, uw, dw)
@@ -61,6 +61,7 @@
     WIDE = [(n * (H // Q), H // Q, 0, C) for n in range(Q)]
     TALL = [[(n * (C // m), C // m, 0, H) for n in range(m)] for m in (NEAR, OUT)]
     TALL.append([(n * (C // FINE), C // FINE, m * W, W) for m in range(2) for n in range(FINE)])
+    ALL = len(TALL[2])
     BASE = [0, len(TALL[0]), len(TALL[0]) + len(TALL[1])]
 
     def part(a, src, half, piece):
@@ -225,13 +226,16 @@
         bh[...] = high
         bl[...] = (blend - high.astype(jnp.float32)).astype(jnp.bfloat16)
 
+    idle = (ps.at[0], ms.at[0], ms.at[1], ms.at[2])
+
     def first_copy(q):
         rows = pl.ds(pl.multiple_of(g * H + q * (H // Q), H // Q), H // Q)
         cols = pl.ds(pl.multiple_of(targets[0][0] * C, C), C)
-        return pltpu.make_async_copy(gt.at[rows, cols], wide.at[0, pl.ds(q * (H // Q), H // Q), :], first.at[q])
-
-    small = [pltpu.make_async_copy(a, b, first.at[Q + n]) for n, (a, b) in enumerate(
-        ((gain_at, gain), (tokens_at, tokens), (routes_at, routes_t), (weight_at, weight_t)))]
+        return pltpu.make_async_copy(gt.at[rows, cols], wide.at[0, pl.ds(q * (H // Q), H // Q), :], idle[q])
+
+    small = [pltpu.make_async_copy(a, b, c) for a, b, c in (
+        (gain_at, gain, ts.at[0]), (tokens_at, tokens, loc.at[3]),
+        (routes_at, routes_t, loc.at[4]), (weight_at, weight_t, loc.at[5]))]
     small[0].start()
     for q in range(Q):
         first_copy(q).start()
@@ -252,6 +256,9 @@
             z_copy(0, 0, WIDE[q - 1], zr.at[0, places[0][0], q - 1]).start()
     stage_copy(3).start()
     for n in range(1, 9):
+        if n == 3:
+            for copy in small[1:]:
+                copy.wait()
         cast(n)
         a, k = tasks[n - 1][:2]
         if n == 1:
@@ -269,8 +276,6 @@
             def _():
                 for pair in ((1, 0), (2, 0), (0, 1), (0, 2), (1, 1), (1, 2)):
                     z_send(*pair, 0)
-    for copy in small[1:]:
-        copy.wait()
     route()
 
     @pl.when(inner == 1)
@@ -318,6 +323,21 @@
         for p in peers:
             p_copy(c, kind, half, chunk, p, t).start()
         ret[slots(t), cols] = pbf[slots(t), cols]
+
+    def spread(c, kind, half, chunk):
+        cols = unit_of(c, half, chunk)
+        for p in peers:
+            p_copy(c, kind, half, chunk, p, t).start()
+        ret[slots(t), cols] = pbf[slots(t), cols]
+
+    def partial_early(half, cut):
+        early[...] = jnp.dot(hid[:, 0:cut], dw[0:cut, unit_of(far_in, half, 1)], preferred_element_type=jnp.float32)
+
+    def partial_late(half, cut):
+        cols = unit_of(far_in, half, 1)
+        value = early[...] + jnp.dot(hid[:, cut:C], dw[cut:C, cols], preferred_element_type=jnp.float32)
+        pbf[:, cols] = value.astype(jnp.bfloat16)
+        spread(far_in, 3, half, 1)
 
     def mix(c, kind, half, chunk=None):
         cols = unit_of(c, half, chunk)
@@ -370,14 +390,15 @@
         forward(*items[n], 0, half_way)
         settle(*items[n - 2])
         forward(*items[n], half_way, Q)
+        if n == 3:
+            forward(2, near, 0, 0, NEAR)
     settle(*items[4])
 
     @pl.when(inner == 0)
     def _():
+        z_send(2, 2, 1)
         z_send(2, 1, 1)
-        z_send(2, 2, 1)
-
-    forward(2, near, 0, 0, NEAR)
+
     settle(*items[5])
     activate()
     partial_out(f, 0, 0)
@@ -401,7 +422,7 @@
         forward_in(0, FINE)
         landed(2, far_out, 1)
         partial_out(far_out, 2, 1 - g)
-        forward_in(FINE, 2 * FINE)
+        forward_in(FINE, ALL)
         share(0, g)
         share(0, 1 - g)
         partial_out(far_in, 3, g)
@@ -416,19 +437,23 @@
         partial_out(far_out, 2, 1 - g)
         forward_in(0, FINE)
         partial_out(far_in, 3, g, 0)
-        forward_in(FINE, FINE + 1)
+        forward_in(FINE, FINE + FINE // 2)
         landed(2, far_in, 2, 0, FINE)
         partial_out(far_in, 3, 1 - g, 0)
-        forward_in(FINE + 1, 2 * FINE)
-        partial_out(far_in, 3, g, 1)
+        forward_in(FINE + FINE // 2, ALL - 1)
         received(shared.at[0], mr.at[2])
         join(0, g)
         join(0, 1 - g)
+        forward_in(ALL - 1, ALL)
+        partial_out(far_in, 3, g, 1)
         received(shared.at[1], mr.at[3])
         join(1, g, 0)
         join(1, 1 - g, 0)
-        landed(2, far_in, 2, FINE, 2 * FINE)
-        partial_out(far_in, 3, 1 - g, 1)
+        cut = (ALL - FINE - 1) * C // FINE // 128 * 128
+        landed(2, far_in, 2, FINE, ALL - 1)
+        partial_early(1 - g, cut)
+        landed(2, far_in, 2, ALL - 1, ALL)
+        partial_late(1 - g, cut)
         join(1, g, 1)
         join(1, 1 - g, 1)
 
@@ -462,7 +487,7 @@
     span = -(-tokens.shape[0] // 128) * 128
     R, FF = gate.shape
     C, D, H = FF // F, F * R, R // 2
-    Q, NEAR, OUT, FINE = 4, 2, 4, 4
+    Q, NEAR, OUT, FINE = 4, 1, 2, 8
     tok, S = tokens.shape[0], EXPERTS * CAP
     bf, f32 = jnp.bfloat16, jnp.float32
     any_spec, vm = pl.BlockSpec(memory_space=pl.ANY), pl.BlockSpec(memory_space=pltpu.VMEM)
@@ -480,11 +505,11 @@
             pltpu.VMEM((3, H, C), f32), pltpu.VMEM((3, C, H), f32),
             pltpu.VMEM((2, F - 1, H, C), bf), pltpu.VMEM((F - 1, C, H), bf),
             pltpu.VMEM((tok, D), bf), pltpu.VMEM((S, D), bf), pltpu.VMEM((tok, S), bf), pltpu.VMEM((tok, S), bf),
-            pltpu.VMEM((S, D), bf),
+            pltpu.VMEM((S, H // 2), f32), pltpu.VMEM((S, D), bf),
             pltpu.VMEM((S, C), f32), pltpu.VMEM((S, C), f32), pltpu.VMEM((S, C), bf),
             pltpu.VMEM((S, D), bf), pltpu.VMEM((S, D), bf), pltpu.VMEM((tok, D), bf), pltpu.VMEM((2, tok, R), bf),
             dma((2,)), dma((2, F - 1, Q)), dma((NEAR + OUT + 2 * FINE,)), dma((3,)), dma((2, F - 1, Q)), dma((NEAR + OUT + 2 * FINE,)), dma((2,)),
-            dma((1,)), dma((5, 2)), dma((3,)), dma((4,)), dma((6,)), dma((Q + 4,)),
+            dma((1,)), dma((5, 2)), dma((3,)), dma((4,)), dma((6,)),
         ],
         compiler_params=pltpu.CompilerParams(collective_id=0, has_side_effects=True, vmem_limit_bytes=42 * 1024 * 1024),
     )(gate, up, down, gain[None, :], tokens, routes.T, weight.T)

time: 210 us -> 209 us (level)
  no operation moved by 1% of the time
where the time goes in v3:
time: 209 us
  Pallas kernels  208 us (100%)
    pallas_call x1, Pallas kernels, exchange(): pl.pallas_call(functools.partial(exchange_kernel, F, T, R, C, Q, NEAR, OU...  202 us
    pallas_call x1, Pallas kernels, exchange(): pl.pallas_call(deliver_kernel, name='deliver', out_shape=(jax.ShapeDtypeS...  6.2 us

profile of v3, /device:TPU:9, one launch (start us, length us, event | category | flops | bytes accessed | tf_op | source)
XLA Modules:
  0.0 208.6 jit_solution(17526635858573923009)
XLA Ops:
  0.6 201.6 %exchange.1 = (bf16[2048,1408]{1,0:T(8,128)(2,1)S(1)}, bf16[2048,1408]{1,0:T(8,128)(2,1)S(1)}, bf16[1408,2048]{1,0:T(8,128)(2,1)S(1)}, f32[192,512]{1,0:T(8,128)S(1)}, bf16[2,192,512]{2,1,0:T(8,128)(2,1)S(1)}) custom-call(f32[512,5632]{1,0:T(8,128)} %bitcast.9, f32[512,5632]{1,0:T(8,128)} %bitcast.10, f32[5632,512]{1,0:T(8,128)} %bitcast.11, ...), custom_call_target="tpu_custom_call" | custom-call | tf_op jit(solution)/shard_map/exchange/pallas_call | solution.py:495
  202.3 6.2 %deliver.1 = (bf16[2048,1408]{1,0:T(8,128)(2,1)}, bf16[2048,1408]{1,0:T(8,128)(2,1)}, bf16[1408,2048]{1,0:T(8,128)(2,1)}, bf16[192,512]{1,0:T(8,128)(2,1)}) custom-call(bf16[2048,1408]{1,0:T(8,128)(2,1)S(1)} %get-tuple-element.13.gw, bf16[2048,1408]{1,0:T(8,128)(2,1)S(1)} %get-tuple-element.14.uw, bf16[1408,2048]{1,0:T(8,128)(2,1)S(1)} %get-tuple-element.15.dw, ...), custom_call_target="tpu_custom_call" | custom-call | tf_op jit(solution)/shard_map/deliver/pallas_call | solution.py:516

commit v4 on v3

--- a/solution.py
+++ b/solution.py
@@ -364,17 +364,25 @@
 
     def stream(a, place):
         if a < 2:
-            return [(piece, zr.at[a, place, q], yr.at[a, place, q]) for q, piece in enumerate(WIDE)]
-        return [(piece, zt.at[BASE[place] + q], yt.at[BASE[place] + q]) for q, piece in enumerate(TALL[place])]
+            return [(piece, zr.at[a, place, q], yr.at[a, place]) for q, piece in enumerate(WIDE)]
+        last = len(TALL[place]) - 1
+        return [(piece, zt.at[BASE[place] + q], yt.at[place + (q >= FINE) + (q == last) if place == 2 else place])
+                for q, piece in enumerate(TALL[place])]
 
     def forward(a, src, place, begin, end):
         for piece, z, y in stream(a, place)[begin:end]:
             z_recv(a, src, piece, z).wait_recv()
             y_copy(a, src, g, piece, y).start()
 
-    def landed(a, src, place, begin=0, end=None):
-        for piece, _, y in stream(a, place)[begin:end]:
-            y_copy(a, src, 1 - g, piece, y).wait_recv()
+    def landed(a, src, place):
+        whole = (0, H, 0, C) if a < 2 else (0, C, 0, H)
+        y_copy(a, src, 1 - g, whole, yr.at[a, place] if a < 2 else yt.at[place]).wait_recv()
+
+    def landed_in(*groups):
+        rows = C - C // FINE
+        for n in groups:
+            piece = ((0, C, 0, W), (0, rows, W, W), (rows, C - rows, W, W))[n]
+            y_copy(2, far_in, 1 - g, piece, yt.at[2 + n]).wait_recv()
 
     def settle(a, src, place):
         landed(a, src, place)
@@ -426,7 +434,7 @@
         share(0, g)
         share(0, 1 - g)
         partial_out(far_in, 3, g)
-        landed(2, far_in, 2)
+        landed_in(0, 1, 2)
         partial_out(far_in, 3, 1 - g)
         share(1, g)
         share(1, 1 - g)
@@ -438,7 +446,7 @@
         forward_in(0, FINE)
         partial_out(far_in, 3, g, 0)
         forward_in(FINE, FINE + FINE // 2)
-        landed(2, far_in, 2, 0, FINE)
+        landed_in(0)
         partial_out(far_in, 3, 1 - g, 0)
         forward_in(FINE + FINE // 2, ALL - 1)
         received(shared.at[0], mr.at[2])
@@ -450,9 +458,9 @@
         join(1, g, 0)
         join(1, 1 - g, 0)
         cut = (ALL - FINE - 1) * C // FINE // 128 * 128
-        landed(2, far_in, 2, FINE, ALL - 1)
+        landed_in(1)
         partial_early(1 - g, cut)
-        landed(2, far_in, 2, ALL - 1, ALL)
+        landed_in(2)
         partial_late(1 - g, cut)
         join(1, g, 1)
         join(1, 1 - g, 1)
@@ -508,7 +516,7 @@
             pltpu.VMEM((S, H // 2), f32), pltpu.VMEM((S, D), bf),
             pltpu.VMEM((S, C), f32), pltpu.VMEM((S, C), f32), pltpu.VMEM((S, C), bf),
             pltpu.VMEM((S, D), bf), pltpu.VMEM((S, D), bf), pltpu.VMEM((tok, D), bf), pltpu.VMEM((2, tok, R), bf),
-            dma((2,)), dma((2, F - 1, Q)), dma((NEAR + OUT + 2 * FINE,)), dma((3,)), dma((2, F - 1, Q)), dma((NEAR + OUT + 2 * FINE,)), dma((2,)),
+            dma((2,)), dma((2, F - 1, Q)), dma((NEAR + OUT + 2 * FINE,)), dma((3,)), dma((2, F - 1)), dma((5,)), dma((2,)),
             dma((1,)), dma((5, 2)), dma((3,)), dma((4,)), dma((6,)),
         ],
         compiler_params=pltpu.CompilerParams(collective_id=0, has_side_effects=True, vmem_limit_bytes=42 * 1024 * 1024),

time: 209 us -> 209 us (level)
  no operation moved by 1% of the time
where the time goes in v4:
time: 209 us; the launch traced here: 208 us
  Pallas kernels  207 us (99%)
    pallas_call x1, Pallas kernels, exchange(): pl.pallas_call(functools.partial(exchange_kernel, F, T, R, C, Q, NEAR, OU...  201 us
    pallas_call x1, Pallas kernels, exchange(): pl.pallas_call(deliver_kernel, name='deliver', out_shape=(jax.ShapeDtypeS...  6.2 us

profile of v4, /device:TPU:9, one launch (start us, length us, event | category | flops | bytes accessed | tf_op | source)
XLA Modules:
  0.0 208.0 jit_solution(7379517822641591021)
XLA Ops:
  0.6 201.0 %exchange.1 = (bf16[2048,1408]{1,0:T(8,128)(2,1)S(1)}, bf16[2048,1408]{1,0:T(8,128)(2,1)S(1)}, bf16[1408,2048]{1,0:T(8,128)(2,1)S(1)}, f32[192,512]{1,0:T(8,128)S(1)}, bf16[2,192,512]{2,1,0:T(8,128)(2,1)S(1)}) custom-call(f32[512,5632]{1,0:T(8,128)} %bitcast.9, f32[512,5632]{1,0:T(8,128)} %bitcast.10, f32[5632,512]{1,0:T(8,128)} %bitcast.11, ...), custom_call_target="tpu_custom_call" | custom-call | tf_op jit(solution)/shard_map/exchange/pallas_call | solution.py:503
  201.7 6.2 %deliver.1 = (bf16[2048,1408]{1,0:T(8,128)(2,1)}, bf16[2048,1408]{1,0:T(8,128)(2,1)}, bf16[1408,2048]{1,0:T(8,128)(2,1)}, bf16[192,512]{1,0:T(8,128)(2,1)}) custom-call(bf16[2048,1408]{1,0:T(8,128)(2,1)S(1)} %get-tuple-element.13.gw, bf16[2048,1408]{1,0:T(8,128)(2,1)S(1)} %get-tuple-element.14.uw, bf16[1408,2048]{1,0:T(8,128)(2,1)S(1)} %get-tuple-element.15.dw, ...), custom_call_target="tpu_custom_call" | custom-call | tf_op jit(solution)/shard_map/deliver/pallas_call | solution.py:524

commit v5 on v4

--- a/solution.py
+++ b/solution.py
@@ -495,7 +495,7 @@
     span = -(-tokens.shape[0] // 128) * 128
     R, FF = gate.shape
     C, D, H = FF // F, F * R, R // 2
-    Q, NEAR, OUT, FINE = 4, 1, 2, 8
+    Q, NEAR, OUT, FINE = 4, 1, 2, C // 128
     tok, S = tokens.shape[0], EXPERTS * CAP
     bf, f32 = jnp.bfloat16, jnp.float32
     any_spec, vm = pl.BlockSpec(memory_space=pl.ANY), pl.BlockSpec(memory_space=pltpu.VMEM)

time: 209 us -> 209 us (level)
  no operation moved by 1% of the time
where the time goes in v5:
time: 209 us
  Pallas kernels  208 us (100%)
    pallas_call x1, Pallas kernels, exchange(): pl.pallas_call(functools.partial(exchange_kernel, F, T, R, C, Q, NEAR, OU...  202 us
    pallas_call x1, Pallas kernels, exchange(): pl.pallas_call(deliver_kernel, name='deliver', out_shape=(jax.ShapeDtypeS...  6.2 us

profile of v5, /device:TPU:9, one launch (start us, length us, event | category | flops | bytes accessed | tf_op | source)
XLA Modules:
  0.0 208.9 jit_solution(7368272276139686719)
XLA Ops:
  0.6 201.9 %exchange.1 = (bf16[2048,1408]{1,0:T(8,128)(2,1)S(1)}, bf16[2048,1408]{1,0:T(8,128)(2,1)S(1)}, bf16[1408,2048]{1,0:T(8,128)(2,1)S(1)}, f32[192,512]{1,0:T(8,128)S(1)}, bf16[2,192,512]{2,1,0:T(8,128)(2,1)S(1)}) custom-call(f32[512,5632]{1,0:T(8,128)} %bitcast.9, f32[512,5632]{1,0:T(8,128)} %bitcast.10, f32[5632,512]{1,0:T(8,128)} %bitcast.11, ...), custom_call_target="tpu_custom_call" | custom-call | tf_op jit(solution)/shard_map/exchange/pallas_call | solution.py:503
  202.6 6.2 %deliver.1 = (bf16[2048,1408]{1,0:T(8,128)(2,1)}, bf16[2048,1408]{1,0:T(8,128)(2,1)}, bf16[1408,2048]{1,0:T(8,128)(2,1)}, bf16[192,512]{1,0:T(8,128)(2,1)}) custom-call(bf16[2048,1408]{1,0:T(8,128)(2,1)S(1)} %get-tuple-element.13.gw, bf16[2048,1408]{1,0:T(8,128)(2,1)S(1)} %get-tuple-element.14.uw, bf16[1408,2048]{1,0:T(8,128)(2,1)S(1)} %get-tuple-element.15.dw, ...), custom_call_target="tpu_custom_call" | custom-call | tf_op jit(solution)/shard_map/deliver/pallas_call | solution.py:524
